TPU v7x, 32 devices: a whole 2x2x4 slice. The times are simulated.
32 devices in a mesh: grp: 2 (over x), fs: 4 (over z), tp: 4 (over y, core).
Axes of the slice: x: 2, y: 2, z: 4, core: 2. Of those that a mesh axis runs over, the one named last changes fastest.
Arguments:
- tokens: bfloat16 [1024, 3584], P(('grp', 'fs')), parts along dimension 0, may hold values from -6 to 6
- norm_gain: float32 [3584], P('fs'), may hold values from 0.1 to 1.9
- up_master: float32 [3584, 14336], P('fs', 'tp'), may hold values from -0.09375 to 0.09375
- down_master: float32 [3584, 14336], P('fs', 'tp'), may hold values from -0.046875 to 0.046875
Outputs:
- up_ready: bfloat16 [7168, 14336], P('grp', 'tp'), parts along dimension 0
- down_ready: bfloat16 [7168, 14336], P('grp', 'tp'), parts along dimension 0
- mixed_out: bfloat16 [1024, 3584], P(('grp', 'fs', 'tp')), parts along dimension 0
There are 2 independent parts, one for each index of `grp`. A program takes and returns all parts, laid end to end along the dimension named above; an argument that names none is the same for every part. Nothing has to cross between parts.
All inputs are finite; a program needn't handle non-finite values.
Results may differ from a plain program's by a relative error of at most 0.024.
Values may be sent and summed in bfloat16 or wider, within the bound.
A program may use at most 192 MiB of HBM per device.

v0:
```python
import jax
import jax.numpy as jnp
from jax import lax
from jax.sharding import PartitionSpec as P


def per_device(tokens, norm_gain, up_master, down_master):
    up_local = (norm_gain[:, None] * up_master).astype(jnp.bfloat16)
    down_local = down_master.astype(jnp.bfloat16)
    values = tokens.astype(jnp.float32)
    square_mean = jnp.mean(values * values, axis=1, keepdims=True)
    normed = (values * lax.rsqrt(square_mean + 1e-06)).astype(jnp.bfloat16)
    up_ready, down_ready = (
        lax.all_gather(up_local, "fs", axis=0, tiled=True),
        lax.all_gather(down_local, "fs", axis=0, tiled=True),
    )
    up_acts = jnp.dot(normed, up_ready, preferred_element_type=jnp.float32)
    hidden = jnp.square(jax.nn.relu(up_acts)).astype(jnp.bfloat16)
    mixed_out = lax.psum_scatter(
        lax.dot_general(
            hidden, down_ready, (((1,), (1,)), ((), ())), preferred_element_type=jnp.float32
        ).astype(jnp.bfloat16),
        "tp",
        scatter_dimension=0,
        tiled=True,
    )
    return (up_ready, down_ready, mixed_out)


def solution(mesh):
    return jax.shard_map(
        per_device,
        mesh=mesh,
        in_specs=(P(("grp", "fs"), None), P("fs"), P("fs", "tp"), P("fs", "tp")),
        out_specs=(P("grp", "tp"), P("grp", "tp"), P(("grp", "fs", "tp"), None)),
        check_vma=False,
    )
```

profile of v0, /device:TPU:0, one launch (start us, length us, event | category | flops | bytes accessed | tf_op | source)
XLA Modules:
  0.0 978.7 jit_solution(14188376748965304761)
XLA Ops:
  7.2 0.0 all-gather.3.cloned.1.call-start
  7.2 9.3 multiply_convert_fusion
  16.5 0.0 all-gather.3.cloned.1.call-update
  16.5 0.0 copy-start
  16.5 0.0 all-gather.5.cloned.1.call-start
  16.6 8.2 convert_element_type.19
  24.8 0.0 all-gather.5.cloned.1.call-update
  24.8 0.0 reduce-scatter.2.cloned.1.call-start
  24.9 0.0 copy-done
  24.9 0.3 fusion.2
  25.1 427.9 %all-gather.3.cloned.1.call-done = bf16[3584,3584]{1,0:T(8,128)(2,1)} async-done(((bf16[896,3584]{1,0:T(8,128)(2,1)}), bf16[3584,3584]{1,0:T(8,128)(2,1)}) %all-gather.3.cloned.1.call-update) | async-done | bytes 25690128 | tf_op jit(solution)/shard_map/all_gather | solution.py:14
  453.0 434.0 %all-gather.5.cloned.1.call-done = bf16[3584,3584]{1,0:T(8,128)(2,1)} async-done(((bf16[896,3584]{1,0:T(8,128)(2,1)}), bf16[3584,3584]{1,0:T(8,128)(2,1)}) %all-gather.5.cloned.1.call-update) | async-done | bytes 25690128 | tf_op jit(solution)/shard_map/all_gather | solution.py:15
  887.0 21.1 %convolution_convert_fusion = bf16[128,3584]{1,0:T(8,128)(2,1)} fusion(bf16[3584,3584]{1,0:T(8,128)(2,1)} %all-gather.5.cloned.1.call-done, bf16[3584,3584]{1,0:T(8,128)(2,1)} %all-gather.3.cloned.1.call-done, bf16[128,3584]{1,0:T(8,128)(2,1)S(1)} %copy-done, f32[128]{0:T(128)S(1)} %add_rsqrt_fusion), kind=kOutput, calls=%fused_computation.4 | convolution fusion | flops 6579879936 | bytes 53215744 | tf_op jit(solution)/shard_map/dot_general | solution.py:20
  908.2 0.0 reduce-scatter.2.cloned.1.call-update
  908.2 22.4 %reduce-scatter.2.cloned.1.call-done = bf16[32,3584]{1,0:T(8,128)(2,1)} async-done(((bf16[128,3584]{1,0:T(8,128)(2,1)}), bf16[32,3584]{1,0:T(8,128)(2,1)}) %reduce-scatter.2.cloned.1.call-update) | async-done | bytes 229392 | tf_op jit(solution)/shard_map/reduce_scatter | solution.py:19
  930.6 20.8 %copy.9 = bf16[3584,3584]{1,0:T(8,128)(2,1)} copy(bf16[3584,3584]{1,0:T(8,128)(2,1)} %all-gather.3.cloned.1.call-done) | data formatting | bytes 51380224
  951.4 20.8 %copy.10 = bf16[3584,3584]{1,0:T(8,128)(2,1)} copy(bf16[3584,3584]{1,0:T(8,128)(2,1)} %all-gather.5.cloned.1.call-done) | data formatting | bytes 51380224
  (1 shorter events, 0.0 us)
Async XLA Ops:
  7.2 445.9 %all-gather.3.cloned.1.call-start = ((), (), s32[]{:S(2)}) async-start(), calls=%async_computation.1 | async-start | bytes 32112640 | tf_op jit(solution)/shard_map/all_gather | solution.py:14
  16.5 8.4 copy-start
  16.5 870.5 %all-gather.5.cloned.1.call-start = ((), (), s32[]{:S(2)}) async-start(), calls=%async_computation.2 | async-start | bytes 32112640 | tf_op jit(solution)/shard_map/all_gather | solution.py:15
  24.8 905.8 %reduce-scatter.2.cloned.1.call-start = ((), (), s32[]{:S(2)}) async-start(), calls=%async_computation.3 | async-start | bytes 1146880 | tf_op jit(solution)/shard_map/reduce_scatter | solution.py:19
Sparse Core Ops, SparseCore 0:
  16.6 436.3 all-gather.2
  455.2 431.8 all-gather.4
  908.3 22.1 reduce-scatter.1
where the time goes:
time: 979 us
  waiting for transfers between devices  884 us (90%)
  local copies, waits for them, and re-layouts  41.6 us (4%)
  matrix products  21.1 us (2%)
  other arithmetic  17.8 us (2%)
  between operations  13.8 us (1%)
    all_gather x1, waiting for transfers between devices, per_device(): lax.all_gather(down_local, 'fs', axis=0, tiled=True)  434 us
    all_gather x1, waiting for transfers between devices, per_device(): lax.all_gather(up_local, 'fs', axis=0, tiled=True)  428 us
    unnamed x4, local copies, waits for them, and re-layouts  41.6 us
    reduce_scatter x1, waiting for transfers between devices, per_device(): lax.psum_scatter(lax.dot_general(hidden, down_ready, (((1,), (1,)), ((),...  22.4 us
    dot_general x1, matrix products, per_device(): lax.dot_general(hidden, down_ready, (((1,), (1,)), ((), ())), preferred_e...  21.1 us
  transfers between devices with their start and end apart: 3, of which 3 were waited for; matrix products, arithmetic and copies ran while one was open for 1% of the time, Pallas kernels for 0%

commit v1 on v0

v1 whole, which is shorter than its diff:
```python
import functools

import jax
import jax.numpy as jnp
from jax import lax
from jax.experimental import pallas as pl
from jax.experimental.pallas import tpu as pltpu
from jax.sharding import PartitionSpec as P

MESH = pl.DeviceIdType.MESH
VMEM_LIMIT = 60 * 1024 * 1024


def chunk_rows(half, width):
    for rows in range(16, half + 1, 16):
        if half % rows == 0 and rows * width * 2 >= 400 * 1024:
            return rows
    return half


def gather_kernel(sizes, gain, up, down, out, wide, narrow, load, store, zs, zr, own_s, xs, xr):
    groups, n, local, rows, count = sizes
    half = local // groups
    per = 2 * count
    g, f, t = lax.axis_index("grp"), lax.axis_index("fs"), lax.axis_index("tp")
    last = n - 1

    def loads(j, m):
        part = lax.rem(g + j, groups)
        master = (up, down)[m]

        def start(i, _):
            q = j * per + m * count + i
            first = pl.multiple_of(part * half + i * rows, 16)
            pltpu.make_async_copy(master.at[pl.ds(first, rows)], wide.at[q], load.at[q]).start()
            return _

        lax.fori_loop(0, count, start, 0)

    for j in range(groups):
        for m in range(2):
            loads(j, m)

    def where(source, part, q):
        m, i = q // count, q % count
        first = pl.multiple_of(source * local + part * half + i * rows, 16)
        return out.at[m, pl.ds(first, rows)]

    def convert(j, q):
        slot = j * per + q
        part = lax.rem(g + j, groups)
        pltpu.make_async_copy(up.at[pl.ds(0, rows)], wide.at[slot], load.at[slot]).wait()

        @pl.when(q < count)
        def _():
            first = pl.multiple_of(part * half + q * rows, 16)
            narrow[slot] = (gain[pl.ds(first, rows)] * wide[slot]).astype(jnp.bfloat16)

        @pl.when(q >= count)
        def _():
            narrow[slot] = wide[slot].astype(jnp.bfloat16)

    def keep(j, q):
        slot = j * per + q
        part = lax.rem(g + j, groups)
        return pltpu.make_async_copy(narrow.at[slot], where(f, part, q), store.at[slot])

    def own(way, q):
        to = f + 1 if way == 0 else f - 1
        return pltpu.make_async_remote_copy(
            narrow.at[q], where(f, g, q), own_s.at[way * per + q], zr.at[way * last * per + q],
            device_id=(g, to, t), device_id_type=MESH)

    def relay(way, k, q):
        source = f - k if way == 0 else f + k
        to = f + 1 if way == 0 else f - 1
        place = where(source, g, q)
        return pltpu.make_async_remote_copy(
            place, place, zs.at[(way * last + k - 1) * per + q], zr.at[(way * last + k) * per + q],
            device_id=(g, to, t), device_id_type=MESH)

    def arrival(way, k, q):
        source = f - k if way == 0 else f + k
        place = where(source, g, q)
        return pltpu.make_async_remote_copy(
            place, place, zs.at[0], zr.at[(way * last + k - 1) * per + q],
            device_id=(g, f, t), device_id_type=MESH)

    def across(j, way, k, q, part):
        source = f - k if way == 0 else f + k
        place = where(source, part, q)
        s = ((j * 2 + way) * last + k - 1) * per + q
        return pltpu.make_async_remote_copy(
            place, place, xs.at[s], xr.at[s],
            device_id=(lax.rem(g + 1 + j, groups), f, t), device_id_type=MESH)

    has = (f < last, f > 0)
    barrier = pltpu.get_barrier_semaphore()
    for way in range(2):
        @pl.when(has[way])
        def _(way=way):
            to = f + 1 if way == 0 else f - 1
            pl.semaphore_signal(barrier, inc=1, device_id=(g, to, t), device_id_type=MESH)
    for j in range(groups - 1):
        pl.semaphore_signal(barrier, inc=1, device_id=(lax.rem(g + 1 + j, groups), f, t), device_id_type=MESH)
    pl.semaphore_wait(barrier, groups - 1 + jnp.minimum(f, 1) + jnp.minimum(last - f, 1))

    def send_own(q):
        for way in range(2):
            @pl.when(has[way])
            def _(way=way):
                own(way, q).start()
        keep(0, q).start()

    def first_step(q, carry):
        convert(0, q)

        @pl.when(q > 0)
        def _():
            send_own(q - 1)
        return carry

    lax.fori_loop(0, per, first_step, 0)
    if groups > 1:
        convert(1, 0)
    send_own(per - 1)

    def step(k, q):
        for way in range(2):
            reach = (k <= f) if way == 0 else (k <= last - f)

            @pl.when(reach)
            def _(way=way):
                arrival(way, k, q).wait_recv()

                @pl.when(has[way])
                def _():
                    relay(way, k, q).start()
                for j in range(groups - 1):
                    across(j, way, k, q, g).start()

    def first_round(q, carry):
        step(1, q)
        for j in range(1, groups):
            if j > 1:
                convert(j, q)

            @pl.when(q + 1 < per)
            def _():
                if j == 1:
                    convert(1, q + 1)
            keep(j, q).start()
        return carry

    lax.fori_loop(0, per, first_round, 0)

    def later(r, carry):
        step(2 + r // per, r % per)
        return carry

    lax.fori_loop(0, (last - 1) * per, later, 0)

    def finish(r, carry):
        k, q = 1 + r // per, r % per
        for way in range(2):
            reach = (k <= f) if way == 0 else (k <= last - f)

            @pl.when(reach)
            def _(way=way):
                @pl.when(has[way])
                def _():
                    relay(way, k, q).wait_send()
                for j in range(groups - 1):
                    sender = lax.rem(g + groups - 1 - j, groups)
                    across(j, way, k, q, g).wait_send()
                    across(j, way, k, q, sender).wait_recv()
        return carry

    def finish_own(q, carry):
        for j in range(groups):
            keep(j, q).wait()
        for way in range(2):
            @pl.when(has[way])
            def _(way=way):
                own(way, q).wait_send()
        return carry

    lax.fori_loop(0, per, finish_own, 0)
    lax.fori_loop(0, last * per, finish, 0)


def gather(groups, n, gain, up, down):
    local, width = up.shape
    half = local // groups
    rows = chunk_rows(half, width)
    count = half // rows
    per = 2 * count
    last = n - 1
    dma = pltpu.SemaphoreType.DMA
    sent = 2 * (n - 1) * local * width * 2
    return pl.pallas_call(
        functools.partial(gather_kernel, (groups, n, local, rows, count)),
        out_shape=jax.ShapeDtypeStruct((2, n * local, width), jnp.bfloat16),
        in_specs=[pl.BlockSpec(memory_space=pltpu.VMEM)] + [pl.BlockSpec(memory_space=pl.ANY)] * 2,
        out_specs=pl.BlockSpec(memory_space=pl.ANY),
        scratch_shapes=[
            pltpu.VMEM((groups * per, rows, width), jnp.float32),
            pltpu.VMEM((groups * per, rows, width), jnp.bfloat16),
            dma((groups * per,)),
            dma((groups * per,)),
            dma((2 * last * per,)),
            dma((2 * last * per,)),
            dma((2 * per,)),
            dma((max(1, groups - 1) * 2 * last * per,)),
            dma((max(1, groups - 1) * 2 * last * per,)),
        ],
        compiler_params=pltpu.CompilerParams(
            collective_id=0, has_side_effects=True, vmem_limit_bytes=VMEM_LIMIT),
        cost_estimate=pl.CostEstimate(flops=0, bytes_accessed=sent, transcendentals=0),
        name="gather_both",
    )(gain[:, None], up, down)


def up_kernel(normed, block, ready, hidden, total):
    step = pl.program_id(0)

    @pl.when(step == 0)
    def _():
        total[...] = jnp.zeros_like(total)

    weights = block[0]
    ready[...] = weights
    total[...] += jnp.dot(normed[0], weights, preferred_element_type=jnp.float32)

    @pl.when(step == pl.num_programs(0) - 1)
    def _():
        hidden[...] = jnp.square(jnp.maximum(total[...], 0.0)).astype(jnp.bfloat16)


def down_kernel(hidden, block, ready, mixed):
    weights = block[0]
    ready[...] = weights
    mixed[0] = lax.dot_general(
        hidden[...], weights, (((1,), (1,)), ((), ())), preferred_element_type=jnp.float32
    ).astype(jnp.bfloat16)


def sum_kernel(tp, part, out, held, send, recv):
    g, f, t = lax.axis_index("grp"), lax.axis_index("fs"), lax.axis_index("tp")
    barrier = pltpu.get_barrier_semaphore()
    for j in range(1, tp):
        pl.semaphore_signal(barrier, inc=1, device_id=(g, f, lax.rem(t + j, tp)), device_id_type=MESH)
    pl.semaphore_wait(barrier, tp - 1)
    copies = []
    for j in range(1, tp):
        to = lax.rem(t + j, tp)
        copy = pltpu.make_async_remote_copy(
            part.at[to], held.at[j - 1], send.at[j - 1], recv.at[j - 1],
            device_id=(g, f, to), device_id_type=MESH)
        copy.start()
        copies.append(copy)
    total = part[t].astype(jnp.float32)
    for j in range(1, tp):
        copies[j - 1].wait()
        total = total + held[j - 1].astype(jnp.float32)
    out[...] = total.astype(jnp.bfloat16)


def per_device(groups, n, tp, tokens, norm_gain, up_master, down_master):
    values = tokens.astype(jnp.float32)
    square_mean = jnp.mean(values * values, axis=1, keepdims=True)
    normed = (values * lax.rsqrt(square_mean + 1e-06)).astype(jnp.bfloat16)
    both = gather(groups, n, norm_gain, up_master, down_master)
    depth, width = both.shape[1:]
    count = tokens.shape[0]
    steps = 8 if depth % (8 * 128) == 0 or depth % (8 * 16) == 0 else 1
    rows = depth // steps
    blocked = normed.reshape(count, steps, rows).transpose(1, 0, 2)
    ready_spec = pl.BlockSpec((rows, width), lambda i: (i, 0))
    weight = jax.ShapeDtypeStruct((depth, width), jnp.bfloat16)
    params = pltpu.CompilerParams(vmem_limit_bytes=VMEM_LIMIT)
    up_ready, hidden = pl.pallas_call(
        up_kernel,
        grid=(steps,),
        in_specs=[
            pl.BlockSpec((1, count, rows), lambda i: (i, 0, 0)),
            pl.BlockSpec((1, rows, width), lambda i: (0, i, 0)),
        ],
        out_specs=[ready_spec, pl.BlockSpec((count, width), lambda i: (0, 0))],
        out_shape=[weight, jax.ShapeDtypeStruct((count, width), jnp.bfloat16)],
        scratch_shapes=[pltpu.VMEM((count, width), jnp.float32)],
        compiler_params=params,
        name="up_pass",
    )(blocked, both)
    down_ready, mixed = pl.pallas_call(
        down_kernel,
        grid=(steps,),
        in_specs=[
            pl.BlockSpec((count, width), lambda i: (0, 0)),
            pl.BlockSpec((1, rows, width), lambda i: (1, i, 0)),
        ],
        out_specs=[ready_spec, pl.BlockSpec((1, count, rows), lambda i: (i, 0, 0))],
        out_shape=[weight, jax.ShapeDtypeStruct((steps, count, rows), jnp.bfloat16)],
        compiler_params=params,
        name="down_pass",
    )(hidden, both)
    share = count // tp
    parts = mixed.transpose(1, 0, 2).reshape(tp, share, depth)
    mixed_out = pl.pallas_call(
        functools.partial(sum_kernel, tp),
        out_shape=jax.ShapeDtypeStruct((share, depth), jnp.bfloat16),
        in_specs=[pl.BlockSpec(memory_space=pltpu.VMEM)],
        out_specs=pl.BlockSpec(memory_space=pltpu.VMEM),
        scratch_shapes=[
            pltpu.VMEM((tp - 1, share, depth), jnp.bfloat16),
            pltpu.SemaphoreType.DMA((tp - 1,)),
            pltpu.SemaphoreType.DMA((tp - 1,)),
        ],
        compiler_params=pltpu.CompilerParams(
            collective_id=1, has_side_effects=True, vmem_limit_bytes=VMEM_LIMIT),
        name="sum_shares",
    )(parts)
    return (up_ready, down_ready, mixed_out)


def solution(mesh):
    groups, n, tp = (mesh.shape[name] for name in ("grp", "fs", "tp"))
    return jax.shard_map(
        functools.partial(per_device, groups, n, tp),
        mesh=mesh,
        in_specs=(P(("grp", "fs"), None), P("fs"), P("fs", "tp"), P("fs", "tp")),
        out_specs=(P("grp", "tp"), P("grp", "tp"), P(("grp", "fs", "tp"), None)),
        check_vma=False,
    )
```

time: 979 us -> 503 us (0.51)
  waiting for transfers between devices: 884 us -> 0 us
  Pallas kernels: 0 us -> 491 us
  local copies, waits for them, and re-layouts: 41.6 us -> 10 us
  matrix products: 21.1 us -> 0 us
  other arithmetic: 17.8 us -> 0.68 us
  between operations: 13.8 us -> 0.67 us
    all_gather x2 -> x0, waiting for transfers between devices: 862 us -> none  [the longest x1 434 us: per_device(): lax.all_gather(down_local, 'fs', axis=0, tiled=True)]
    pallas_call x0 -> x4, Pallas kernels: none -> 491 us  [the longest x1 435 us: gather(): pl.pallas_call(functools.partial(gather_kernel, (groups, n, local, rows,...]
    unnamed x4 -> x2, local copies, waits for them, and re-layouts: 41.6 us -> 3.2 us
    reduce_scatter x1 -> x0, waiting for transfers between devices: 22.4 us -> none  [per_device(): lax.psum_scatter(lax.dot_general(hidden, down_ready, (((1,), (1,)), ((),...]
    dot_general x1 -> x0, matrix products: 21.1 us -> none  [per_device(): lax.dot_general(hidden, down_ready, (((1,), (1,)), ((), ())), preferred_e...]
    convert_element_type x2 -> x1, other arithmetic: 17.5 us -> 0.18 us  [per_device(): normed = (values * lax.rsqrt(square_mean + 1e-06)).astype(jnp.bfloat16)]
  transfers between devices with their start and end apart: 3 -> 0, of which waited for: 3 -> 0; matrix products, arithmetic and copies ran while one was open for 1% -> 0% of each run, Pallas kernels for 0% -> 0%
where the time goes in v1:
time: 503 us; the launch traced here: 502 us
  Pallas kernels  491 us (98%)
  local copies, waits for them, and re-layouts  10 us (2%)
    pallas_call x1, Pallas kernels, gather(): pl.pallas_call(functools.partial(gather_kernel, (groups, n, local, rows,...  435 us
    pallas_call x1, Pallas kernels, per_device(): pl.pallas_call(down_kernel, grid=(steps,), in_specs=[pl.BlockSpec((count,...  21.5 us
    pallas_call x1, Pallas kernels, per_device(): pl.pallas_call(up_kernel, grid=(steps,), in_specs=[pl.BlockSpec((1, count...  20.9 us
    pallas_call x1, Pallas kernels, per_device(): pl.pallas_call(functools.partial(sum_kernel, tp), out_shape=jax.ShapeDtyp...  13.8 us

profile of v1, /device:TPU:0, one launch (start us, length us, event | category | flops | bytes accessed | tf_op | source)
XLA Modules:
  0.0 502.3 jit_solution(15163793809400323177)
XLA Ops:
  0.6 1.6 copy.8
  2.2 0.5 fusion
  2.7 0.2 fusion.1
  2.9 1.3 copy.9
  4.2 1.6 broadcast_in_dim.5.gain
  5.8 434.7 %gather_both.1.block = bf16[2,3584,3584]{2,1,0:T(8,128)(2,1)} custom-call(f32[896,1]{1,0:T(8,128)} %broadcast_in_dim.5.gain, f32[896,3584]{1,0:T(8,128)} %up.1, f32[896,3584]{1,0:T(8,128)} %down.1), custom_call_target="tpu_custom_call" | custom-call | bytes 38535168 | tf_op jit(solution)/shard_map/gather_both/pallas_call | solution.py:201
  440.5 20.9 %up_pass.1 = (bf16[3584,3584]{1,0:T(8,128)(2,1)}, bf16[128,3584]{1,0:T(8,128)(2,1)}) custom-call(bf16[8,128,448]{2,1,0:T(8,128)(2,1)} %bitcast.3, bf16[2,3584,3584]{2,1,0:T(8,128)(2,1)} %gather_both.1.block), custom_call_target="tpu_custom_call" | custom-call | tf_op jit(solution)/shard_map/up_pass/pallas_call | solution.py:282
  461.5 21.5 %down_pass.1 = (bf16[3584,3584]{1,0:T(8,128)(2,1)}, bf16[8,128,448]{2,1,0:T(8,128)(2,1)}) custom-call(bf16[128,3584]{1,0:T(8,128)(2,1)} %get-tuple-element.8.hidden, bf16[2,3584,3584]{2,1,0:T(8,128)(2,1)} %gather_both.1.block), custom_call_target="tpu_custom_call" | custom-call | tf_op jit(solution)/shard_map/down_pass/pallas_call | solution.py:295
  483.0 1.8 copy.11
  484.8 2.1 reshape.21.part
  486.8 13.8 %sum_shares.1 = bf16[32,3584]{1,0:T(8,128)(2,1)} custom-call(bf16[4,32,3584]{2,1,0:T(8,128)(2,1)} %reshape.21.part), custom_call_target="tpu_custom_call" | custom-call | tf_op jit(solution)/shard_map/sum_shares/pallas_call | solution.py:309
  500.7 1.6 copy.13
  (1 shorter events, 0.0 us)

commit v2 on v1

--- a/solution.py
+++ b/solution.py
@@ -9,11 +9,12 @@
 
 MESH = pl.DeviceIdType.MESH
 VMEM_LIMIT = 60 * 1024 * 1024
+ROWS = 512
 
 
 def chunk_rows(half, width):
     for rows in range(16, half + 1, 16):
-        if half % rows == 0 and rows * width * 2 >= 400 * 1024:
+        if half % rows == 0 and rows * width * 2 >= 200 * 1024:
             return rows
     return half
 
@@ -221,105 +222,119 @@
     )(gain[:, None], up, down)
 
 
-def up_kernel(normed, block, ready, hidden, total):
+def pass_kernel(steps, tokens, block, up_ready, down_ready, mixed, normed, total, hidden):
     step = pl.program_id(0)
+    rows = block.shape[1]
 
     @pl.when(step == 0)
     def _():
+        values = tokens[...].astype(jnp.float32)
+        square_mean = jnp.mean(values * values, axis=1, keepdims=True)
+        scaled = (values * lax.rsqrt(square_mean + 1e-06)).astype(jnp.bfloat16)
+        for i in range(steps):
+            normed[i] = scaled[:, i * rows:(i + 1) * rows]
         total[...] = jnp.zeros_like(total)
 
-    weights = block[0]
-    ready[...] = weights
-    total[...] += jnp.dot(normed[0], weights, preferred_element_type=jnp.float32)
-
-    @pl.when(step == pl.num_programs(0) - 1)
+    @pl.when(step < steps)
+    def _():
+        weights = block[0]
+        up_ready[...] = weights
+        total[...] += jnp.dot(normed[step], weights, preferred_element_type=jnp.float32)
+
+    @pl.when(step == steps - 1)
     def _():
         hidden[...] = jnp.square(jnp.maximum(total[...], 0.0)).astype(jnp.bfloat16)
 
-
-def down_kernel(hidden, block, ready, mixed):
-    weights = block[0]
-    ready[...] = weights
-    mixed[0] = lax.dot_general(
-        hidden[...], weights, (((1,), (1,)), ((), ())), preferred_element_type=jnp.float32
-    ).astype(jnp.bfloat16)
-
-
-def sum_kernel(tp, part, out, held, send, recv):
+    @pl.when(step >= steps)
+    def _():
+        weights = block[0]
+        down_ready[...] = weights
+        mixed[...] = lax.dot_general(
+            hidden[...], weights, (((1,), (1,)), ((), ())), preferred_element_type=jnp.float32
+        ).astype(jnp.bfloat16)
+
+
+def sum_kernel(chips, part, out, pair, near, far, send, recv):
     g, f, t = lax.axis_index("grp"), lax.axis_index("fs"), lax.axis_index("tp")
+    y, c = t // 2, lax.rem(t, 2)
+    sibling = (g, f, 2 * y + 1 - c)
+
+    def other(j):
+        return lax.rem(y + j, chips)
+
     barrier = pltpu.get_barrier_semaphore()
-    for j in range(1, tp):
-        pl.semaphore_signal(barrier, inc=1, device_id=(g, f, lax.rem(t + j, tp)), device_id_type=MESH)
-    pl.semaphore_wait(barrier, tp - 1)
-    copies = []
-    for j in range(1, tp):
-        to = lax.rem(t + j, tp)
+    pl.semaphore_signal(barrier, inc=1, device_id=sibling, device_id_type=MESH)
+    for j in range(1, chips):
+        pl.semaphore_signal(barrier, inc=1, device_id=(g, f, 2 * other(j) + c), device_id_type=MESH)
+    pl.semaphore_wait(barrier, chips)
+    over, back = [], []
+    for j in list(range(1, chips)) + [0]:
         copy = pltpu.make_async_remote_copy(
-            part.at[to], held.at[j - 1], send.at[j - 1], recv.at[j - 1],
-            device_id=(g, f, to), device_id_type=MESH)
+            part.at[2 * other(j) + 1 - c], near.at[j], send.at[j], recv.at[j],
+            device_id=sibling, device_id_type=MESH)
         copy.start()
-        copies.append(copy)
-    total = part[t].astype(jnp.float32)
-    for j in range(1, tp):
-        copies[j - 1].wait()
-        total = total + held[j - 1].astype(jnp.float32)
+        over.append((j, copy))
+    for j, copy in over:
+        copy.wait_recv()
+        both = part[2 * other(j) + c].astype(jnp.float32) + near[j].astype(jnp.float32)
+        if j == 0:
+            total = both
+        else:
+            pair[j] = both.astype(jnp.bfloat16)
+            copy = pltpu.make_async_remote_copy(
+                pair.at[j], far.at[j], send.at[chips + j], recv.at[chips + j],
+                device_id=(g, f, 2 * other(j) + c), device_id_type=MESH)
+            copy.start()
+            back.append((j, copy))
+    for j, copy in back:
+        copy.wait_recv()
+        total = total + far[j].astype(jnp.float32)
     out[...] = total.astype(jnp.bfloat16)
+    for _, copy in over + back:
+        copy.wait_send()
 
 
 def per_device(groups, n, tp, tokens, norm_gain, up_master, down_master):
-    values = tokens.astype(jnp.float32)
-    square_mean = jnp.mean(values * values, axis=1, keepdims=True)
-    normed = (values * lax.rsqrt(square_mean + 1e-06)).astype(jnp.bfloat16)
     both = gather(groups, n, norm_gain, up_master, down_master)
     depth, width = both.shape[1:]
     count = tokens.shape[0]
-    steps = 8 if depth % (8 * 128) == 0 or depth % (8 * 16) == 0 else 1
-    rows = depth // steps
-    blocked = normed.reshape(count, steps, rows).transpose(1, 0, 2)
-    ready_spec = pl.BlockSpec((rows, width), lambda i: (i, 0))
+    rows = next(size for size in (ROWS, 256, 128, depth) if depth % size == 0)
+    steps = depth // rows
     weight = jax.ShapeDtypeStruct((depth, width), jnp.bfloat16)
-    params = pltpu.CompilerParams(vmem_limit_bytes=VMEM_LIMIT)
-    up_ready, hidden = pl.pallas_call(
-        up_kernel,
-        grid=(steps,),
+    up_ready, down_ready, mixed = pl.pallas_call(
+        functools.partial(pass_kernel, steps),
+        grid=(2 * steps,),
         in_specs=[
-            pl.BlockSpec((1, count, rows), lambda i: (i, 0, 0)),
-            pl.BlockSpec((1, rows, width), lambda i: (0, i, 0)),
+            pl.BlockSpec((count, depth), lambda i: (0, 0)),
+            pl.BlockSpec((1, rows, width), lambda i: (i // steps, i % steps, 0)),
         ],
-        out_specs=[ready_spec, pl.BlockSpec((count, width), lambda i: (0, 0))],
-        out_shape=[weight, jax.ShapeDtypeStruct((count, width), jnp.bfloat16)],
-        scratch_shapes=[pltpu.VMEM((count, width), jnp.float32)],
-        compiler_params=params,
-        name="up_pass",
-    )(blocked, both)
-    down_ready, mixed = pl.pallas_call(
-        down_kernel,
-        grid=(steps,),
-        in_specs=[
-            pl.BlockSpec((count, width), lambda i: (0, 0)),
-            pl.BlockSpec((1, rows, width), lambda i: (1, i, 0)),
+        out_specs=[
+            pl.BlockSpec((rows, width), lambda i: (jnp.minimum(i, steps - 1), 0)),
+            pl.BlockSpec((rows, width), lambda i: (jnp.maximum(i - steps, 0), 0)),
+            pl.BlockSpec((count, rows), lambda i: (0, jnp.maximum(i - steps, 0))),
         ],
-        out_specs=[ready_spec, pl.BlockSpec((1, count, rows), lambda i: (i, 0, 0))],
-        out_shape=[weight, jax.ShapeDtypeStruct((steps, count, rows), jnp.bfloat16)],
-        compiler_params=params,
-        name="down_pass",
-    )(hidden, both)
+        out_shape=[weight, weight, jax.ShapeDtypeStruct((count, depth), jnp.bfloat16)],
+        scratch_shapes=[
+            pltpu.VMEM((steps, count, rows), jnp.bfloat16),
+            pltpu.VMEM((count, width), jnp.float32),
+            pltpu.VMEM((count, width), jnp.bfloat16),
+        ],
+        compiler_params=pltpu.CompilerParams(vmem_limit_bytes=VMEM_LIMIT),
+        name="both_passes",
+    )(tokens, both)
     share = count // tp
-    parts = mixed.transpose(1, 0, 2).reshape(tp, share, depth)
+    chips = tp // 2
+    held = pltpu.VMEM((chips, share, depth), jnp.bfloat16)
     mixed_out = pl.pallas_call(
-        functools.partial(sum_kernel, tp),
+        functools.partial(sum_kernel, chips),
         out_shape=jax.ShapeDtypeStruct((share, depth), jnp.bfloat16),
         in_specs=[pl.BlockSpec(memory_space=pltpu.VMEM)],
         out_specs=pl.BlockSpec(memory_space=pltpu.VMEM),
-        scratch_shapes=[
-            pltpu.VMEM((tp - 1, share, depth), jnp.bfloat16),
-            pltpu.SemaphoreType.DMA((tp - 1,)),
-            pltpu.SemaphoreType.DMA((tp - 1,)),
-        ],
+        scratch_shapes=[held, held, held] + [pltpu.SemaphoreType.DMA((2 * chips,))] * 2,
         compiler_params=pltpu.CompilerParams(
             collective_id=1, has_side_effects=True, vmem_limit_bytes=VMEM_LIMIT),
         name="sum_shares",
-    )(parts)
+    )(mixed.reshape(tp, share, depth))
     return (up_ready, down_ready, mixed_out)
 
 

time: 503 us -> 493 us (0.980)
  local copies, waits for them, and re-layouts: 10 us -> 3.28 us
    pallas_call x3 -> x2, Pallas kernels: 56.3 us -> 54.2 us  [the longest x1 42.9 us: per_device(): pl.pallas_call(functools.partial(pass_kernel, steps), grid=(2 * steps,),...]
where the time goes in v2:
time: 493 us; the launch traced here: 492 us
  Pallas kernels  488 us (99%)
    pallas_call x1, Pallas kernels, gather(): pl.pallas_call(functools.partial(gather_kernel, (groups, n, local, rows,...  434 us
    pallas_call x1, Pallas kernels, per_device(): pl.pallas_call(functools.partial(pass_kernel, steps), grid=(2 * steps,),...  42.9 us
    pallas_call x1, Pallas kernels, per_device(): pl.pallas_call(functools.partial(sum_kernel, chips), out_shape=jax.ShapeD...  11.3 us

profile of v2, /device:TPU:0, one launch (start us, length us, event | category | flops | bytes accessed | tf_op | source)
XLA Modules:
  0.0 492.2 jit_solution(4575094930089935217)
XLA Ops:
  0.6 1.6 broadcast_in_dim.4.gain
  2.3 434.1 %gather_both.1.block = bf16[2,3584,3584]{2,1,0:T(8,128)(2,1)} custom-call(f32[896,1]{1,0:T(8,128)} %broadcast_in_dim.4.gain, f32[896,3584]{1,0:T(8,128)} %up.1, f32[896,3584]{1,0:T(8,128)} %down.1), custom_call_target="tpu_custom_call" | custom-call | bytes 38535168 | tf_op jit(solution)/shard_map/gather_both/pallas_call | solution.py:202
  436.4 42.9 %both_passes.1 = (bf16[3584,3584]{1,0:T(8,128)(2,1)}, bf16[3584,3584]{1,0:T(8,128)(2,1)}, bf16[128,3584]{1,0:T(8,128)(2,1)}) custom-call(bf16[128,3584]{1,0:T(8,128)(2,1)} %tokens.1, bf16[2,3584,3584]{2,1,0:T(8,128)(2,1)} %gather_both.1.block), custom_call_target="tpu_custom_call" | custom-call | tf_op jit(solution)/shard_map/both_passes/pallas_call | solution.py:304
  479.3 11.3 %sum_shares.1 = bf16[32,3584]{1,0:T(8,128)(2,1)} custom-call(bf16[4,32,3584]{2,1,0:T(8,128)(2,1)} %bitcast.1), custom_call_target="tpu_custom_call" | custom-call | tf_op jit(solution)/shard_map/sum_shares/pallas_call | solution.py:328
  490.6 1.6 copy.9
